TPU v7x, 32 devices: a whole 2x2x4 slice. The times are simulated.
32 devices in a mesh: sp: 4 (over z), fs: 4 (over y, x), tp: 2 (over core).
Axes of the slice: x: 2, y: 2, z: 4, core: 2. Of those that a mesh axis runs over, the one named last changes fastest.
Arguments:
- tokens: bfloat16 [1024, 2048], P('sp', ('fs', 'tp')), may hold values from -500 to 500
- norm_gain: float32 [2048], replicated, may hold values from 0.1 to 1.9
- query_w: bfloat16 [2048, 1024], P('sp', ('fs', 'tp')), may hold values from -1 to 1
- key_w: bfloat16 [2048, 512], P('sp', ('fs', 'tp')), may hold values from -1 to 1
- value_w: bfloat16 [2048, 512], P('sp', ('fs', 'tp')), may hold values from -0.125 to 0.125
- recept_w: bfloat16 [2048, 1024], P('sp', ('fs', 'tp')), may hold values from -0.125 to 0.125
- rec_key_w: bfloat16 [2048, 1024], P('sp', ('fs', 'tp')), may hold values from -0.125 to 0.125
- rec_value_w: bfloat16 [2048, 1024], P('sp', ('fs', 'tp')), may hold values from -0.125 to 0.125
- decay_down: bfloat16 [2048, 64], replicated, may hold values from -0.125 to 0.125
- decay_up: bfloat16 [64, 1024], replicated, may hold values from -1 to 1
- decay_base: float32 [16, 1024], P(('fs', 'tp'), 'sp'), may hold values from -14 to 0
- learn_rate: float32 [1024], P(('fs', 'tp')), may hold values from 0.1 to 1
- query_gain: float32 [64], replicated, may hold values from 0 to 7
- key_gain: float32 [64], replicated, may hold values from 0 to 7
- sink_logit: float32 [16], P(('fs', 'tp')), may hold values from 1 to 5
- group_gain: float32 [1024], P(('fs', 'tp')), may hold values from 0.1 to 1.9
- out_att_w: bfloat16 [1024, 2048], P(('fs', 'tp'), 'sp'), may hold values from -0.75 to 0.75
- out_rec_w: bfloat16 [1024, 2048], P(('fs', 'tp'), 'sp'), may hold values from -0.1875 to 0.1875
Outputs:
- mixed: bfloat16 [1024, 2048], P(('sp', 'fs', 'tp'))
- row_lse: float32 [16, 1024], P(('fs', 'tp'), 'sp')
All inputs are finite; a program needn't handle non-finite values.
Results may differ from a plain program's by a relative error of at most 0.015.
Values may be sent and summed in bfloat16 or wider, within the bound.
A program may use at most 64 MiB of HBM per device.

v0:
```python
import math

import jax
import jax.numpy as jnp
from jax import lax
from jax.sharding import PartitionSpec as P

HEAD = 64
WINDOW = 128
BLOCK = 32


NORM_EPS = 1e-06
KEY_EPS = 1e-06
GROUP_EPS = 0.00064
EXACT_PRECISION = lax.Precision.HIGHEST


def passed_along(array, axis, by):
    devices = lax.axis_size(axis)
    pairs = [(i, i + by) for i in range(devices) if 0 <= i + by < devices]
    return lax.ppermute(array, axis, pairs)


def prefix(array, axis, combine, identity):
    devices, place = (lax.axis_size(axis), lax.axis_index(axis))
    everything = lax.all_gather(array.astype(jnp.bfloat16), axis)
    start = jnp.broadcast_to(jnp.asarray(identity, array.dtype), array.shape)

    def turn(k, before):
        reached = k < place
        new = combine(before, everything[k].astype(array.dtype))
        return jnp.where(reached, new, before)

    return lax.fori_loop(0, devices, turn, start)


def head_rms(values, gain_vec, num_heads):
    shaped = values.astype(jnp.float32).reshape(values.shape[0], num_heads, HEAD)
    mean_sq = jnp.mean(shaped * shaped, axis=-1, keepdims=True)
    return (shaped * lax.rsqrt(mean_sq + NORM_EPS) * gain_vec).astype(jnp.bfloat16)


def attend(query_rows, key_rows, value_rows, query_gain, key_gain, sink_logit):
    num_rows = query_rows.shape[0]
    num_heads = query_rows.shape[1] // HEAD
    kv_heads = key_rows.shape[1] // HEAD
    group_size = num_heads // kv_heads
    blocks = num_rows // WINDOW
    query_n = head_rms(query_rows, query_gain, num_heads).reshape(
        blocks, WINDOW, kv_heads, group_size, HEAD
    )
    key_n = head_rms(key_rows, key_gain, kv_heads).reshape(num_rows, kv_heads * HEAD)
    paired = jnp.concatenate([key_n, value_rows], axis=1)
    before = passed_along(paired[num_rows - WINDOW :], "sp", 1)
    current = paired.reshape(blocks, WINDOW, 2 * kv_heads * HEAD)
    previous = jnp.concatenate([before[None], current[:-1]], axis=0)
    key_band = jnp.concatenate([previous, current], axis=1).reshape(
        blocks, 2 * WINDOW, 2, kv_heads, HEAD
    )
    scores = jnp.einsum(
        "nqkgd,nskd->nkgqs", query_n, key_band[:, :, 0], preferred_element_type=jnp.float32
    ) * (1.0 / math.sqrt(HEAD))
    offset = lax.axis_index("sp") * num_rows
    lag_table = (
        lax.broadcasted_iota(jnp.int32, (WINDOW, 2 * WINDOW), 0)
        + WINDOW
        - lax.broadcasted_iota(jnp.int32, (WINDOW, 2 * WINDOW), 1)
    )
    key_place = (
        offset
        + (lax.broadcasted_iota(jnp.int32, (blocks, 2 * WINDOW), 0) - 1) * WINDOW
        + lax.broadcasted_iota(jnp.int32, (blocks, 2 * WINDOW), 1)
    )
    allowed = ((lag_table >= 0) & (lag_table < WINDOW))[None, :, :] & (key_place >= 0)[:, None, :]
    allowed = allowed[:, None, None]
    sink_cols = sink_logit.reshape(kv_heads, group_size)[None, :, :, None, None]
    masked = jnp.where(allowed, scores, -jnp.inf)
    row_top = jnp.maximum(jnp.max(masked, axis=-1, keepdims=True), sink_cols)
    weight = jnp.where(allowed, jnp.exp(masked - row_top), 0.0)
    row_total = jnp.sum(weight, axis=-1, keepdims=True) + jnp.exp(sink_cols - row_top)
    row_lse = (
        (row_top + jnp.log(row_total))[..., 0].transpose(1, 2, 0, 3).reshape(num_heads, num_rows)
    )
    att_probs = (weight / row_total).astype(jnp.bfloat16)
    mixed_heads = jnp.einsum(
        "nkgqs,nskd->nqkgd", att_probs, key_band[:, :, 1], preferred_element_type=jnp.float32
    )
    return (mixed_heads.reshape(num_rows, num_heads * HEAD).astype(jnp.bfloat16), row_lse)


def unit_inverse(lower_mat):
    mat_size = lower_mat.shape[-1]
    result = jnp.eye(mat_size, dtype=jnp.float32) + lower_mat
    power_mat = lower_mat
    for section_index in range(mat_size.bit_length() - 2):
        power_mat = jnp.einsum("hij,hjk->hik", power_mat, power_mat, precision=EXACT_PRECISION)
        result = result + jnp.einsum("hij,hjk->hik", result, power_mat, precision=EXACT_PRECISION)
    return result


def pair_table(left_vals, right_vals, allowed):
    return jnp.where(
        allowed, jnp.einsum("hid,hjd->hij", left_vals, right_vals, precision=EXACT_PRECISION), 0.0
    )


def recur(reads, rec_keys, rec_values, log_decay, learn_rate, group_gain):
    num_rows = reads.shape[0]
    num_heads = reads.shape[1] // HEAD
    blocks = num_rows // BLOCK

    def by_block(values):
        return (
            values.astype(jnp.float32).reshape(blocks, BLOCK, num_heads, HEAD).transpose(0, 2, 1, 3)
        )

    read_vals = by_block(reads)
    key_vals = by_block(rec_keys)
    value_vals = by_block(rec_values)
    decay_vals = by_block(log_decay)
    unit_key = key_vals * lax.rsqrt(jnp.sum(key_vals * key_vals, axis=-1, keepdims=True) + KEY_EPS)
    removal = -unit_key
    writing = unit_key * learn_rate.reshape(num_heads, HEAD)[None, :, None, :]
    stacked = jnp.concatenate([jnp.zeros_like(value_vals), value_vals], axis=-1)
    unit_matrix = jnp.broadcast_to(jnp.eye(HEAD, dtype=jnp.float32), (num_heads, HEAD, HEAD))
    start_pair = jnp.concatenate(
        [unit_matrix, jnp.zeros((num_heads, HEAD, HEAD), jnp.float32)], axis=1
    )
    row_iota = lax.broadcasted_iota(jnp.int32, (BLOCK, BLOCK), 0)
    col_iota = lax.broadcasted_iota(jnp.int32, (BLOCK, BLOCK), 1)
    strict = (row_iota > col_iota)[None]
    inclusive = (row_iota >= col_iota)[None]

    def block_step(state_per_block, inputs):
        read_now, key_now, removal_now, writing_now, decay_now, current_value = inputs
        cum_decay = jnp.cumsum(decay_now, axis=1)
        decay_matrix_a = removal_now * jnp.exp(cum_decay - decay_now)
        decay_matrix_b = writing_now * jnp.exp(-cum_decay)
        stacked_key_matrix = key_now * jnp.exp(-cum_decay)
        stacked_receptance = read_now * jnp.exp(cum_decay)
        m_ab = pair_table(decay_matrix_a, decay_matrix_b, strict)
        m_ak = pair_table(decay_matrix_a, stacked_key_matrix, strict)
        m_rb = pair_table(stacked_receptance, decay_matrix_b, inclusive)
        m_rk = pair_table(stacked_receptance, stacked_key_matrix, inclusive)
        right_operand = jnp.einsum(
            "bvq,bzq->bvz", decay_matrix_a, state_per_block, precision=EXACT_PRECISION
        ) + jnp.einsum("hij,hjm->him", m_ak, current_value, precision=EXACT_PRECISION)
        delta_updates = jnp.einsum(
            "hij,hjm->him", unit_inverse(m_ab), right_operand, precision=EXACT_PRECISION
        )
        block_out = (
            jnp.einsum(
                "bvq,bzq->bvz", stacked_receptance, state_per_block, precision=EXACT_PRECISION
            )
            + jnp.einsum("hij,hjm->him", m_rb, delta_updates, precision=EXACT_PRECISION)
            + jnp.einsum("hij,hjm->him", m_rk, current_value, precision=EXACT_PRECISION)
        )
        grown_state = (
            state_per_block
            + jnp.einsum("sao,sac->soc", delta_updates, decay_matrix_b, precision=EXACT_PRECISION)
            + jnp.einsum(
                "sao,sac->soc", current_value, stacked_key_matrix, precision=EXACT_PRECISION
            )
        )
        return (grown_state * jnp.exp(cum_decay[:, -1])[:, None, :], block_out)

    final_state, block_outs = lax.scan(
        block_step, start_pair, (read_vals, key_vals, removal, writing, decay_vals, stacked)
    )

    def chain(earlier, later_pair):
        moved_state = jnp.einsum(
            "hmk,hkj->hmj", earlier, later_pair[:, :HEAD], precision=EXACT_PRECISION
        )
        return moved_state + jnp.concatenate(
            [jnp.zeros_like(later_pair[:, HEAD:]), later_pair[:, HEAD:]], axis=1
        )

    carried = prefix(final_state, "sp", chain, start_pair)
    incoming = carried[:, HEAD:]
    result = block_outs[..., HEAD:] + jnp.einsum(
        "nhlm,hvm->nhlv", block_outs[..., :HEAD], incoming, precision=EXACT_PRECISION
    )
    mean_val = jnp.mean(result, axis=-1, keepdims=True)
    centered = result - mean_val
    variance = jnp.mean(centered * centered, axis=-1, keepdims=True)
    normed = (
        (centered * lax.rsqrt(variance + GROUP_EPS))
        .transpose(0, 2, 1, 3)
        .reshape(num_rows, num_heads * HEAD)
    )
    return (normed * group_gain).astype(jnp.bfloat16)


def per_device(
    tokens,
    norm_gain,
    query_w,
    key_w,
    value_w,
    recept_w,
    rec_key_w,
    rec_value_w,
    decay_down,
    decay_up,
    decay_base,
    learn_rate,
    query_gain,
    key_gain,
    sink_logit,
    group_gain,
    out_att_w,
    out_rec_w,
):
    groups = lax.axis_size(("fs", "tp"))
    own_width = tokens.shape[1]
    own_values = tokens.astype(jnp.float32)
    squares = lax.psum(jnp.sum(own_values * own_values, axis=1), ("fs", "tp"))
    gain_part = lax.dynamic_slice_in_dim(
        norm_gain, lax.axis_index(("fs", "tp")) * own_width, own_width, 0
    )
    scaled = own_values * lax.rsqrt(squares / (own_width * groups) + NORM_EPS)[:, None] * gain_part
    outgoing = scaled.astype(jnp.bfloat16)
    gathered = lax.all_gather(outgoing, ("fs", "tp"), axis=1, tiled=True)

    def rounded(sums):
        return lax.optimization_barrier(
            tuple((acc_total.astype(jnp.bfloat16) for acc_total in sums))
        )

    rec_span = recept_w.shape[1]
    decay_cols = lax.dynamic_slice_in_dim(
        decay_up, lax.axis_index(("fs", "tp")) * rec_span, rec_span, 1
    )
    decay_low = jnp.tanh(jnp.dot(gathered, decay_down, preferred_element_type=jnp.float32)).astype(
        jnp.bfloat16
    )
    decay_rate = jnp.dot(decay_low, decay_cols, preferred_element_type=jnp.float32) + jnp.repeat(
        decay_base.T, HEAD, axis=1
    )
    log_decay = -jnp.exp(decay_rate)
    pieces = (
        lax.all_gather(query_w, "sp", axis=0, tiled=True),
        lax.all_gather(key_w, "sp", axis=0, tiled=True),
        lax.all_gather(value_w, "sp", axis=0, tiled=True),
        lax.all_gather(recept_w, "sp", axis=0, tiled=True),
        lax.all_gather(rec_key_w, "sp", axis=0, tiled=True),
        lax.all_gather(rec_value_w, "sp", axis=0, tiled=True),
    )
    all_sums = tuple(
        (
            jnp.dot(gathered, weight_piece, preferred_element_type=jnp.float32)
            for weight_piece in pieces
        )
    )
    att_inputs = rounded(all_sums[:3])
    att_mix, row_lse = attend(
        att_inputs[0], att_inputs[1], att_inputs[2], query_gain, key_gain, sink_logit
    )
    rec_sums = all_sums[3:]
    rec_inputs = rounded(rec_sums)
    rec_mix = recur(rec_inputs[0], rec_inputs[1], rec_inputs[2], log_decay, learn_rate, group_gain)
    att_full, rec_full = (
        lax.all_gather(out_att_w, "sp", axis=1, tiled=True),
        lax.all_gather(out_rec_w, "sp", axis=1, tiled=True),
    )
    mixed_out = lax.psum_scatter(
        (
            jnp.dot(att_mix, att_full, preferred_element_type=jnp.float32)
            + jnp.dot(rec_mix, rec_full, preferred_element_type=jnp.float32)
        ).astype(jnp.bfloat16),
        ("fs", "tp"),
        scatter_dimension=0,
        tiled=True,
    )
    return (mixed_out, row_lse)


def solution(mesh):
    in_specs = (
        P("sp", ("fs", "tp")),
        P(),
        P("sp", ("fs", "tp")),
        P("sp", ("fs", "tp")),
        P("sp", ("fs", "tp")),
        P("sp", ("fs", "tp")),
        P("sp", ("fs", "tp")),
        P("sp", ("fs", "tp")),
        P(),
        P(),
        P(("fs", "tp"), "sp"),
        P(("fs", "tp")),
        P(),
        P(),
        P(("fs", "tp")),
        P(("fs", "tp")),
        P(("fs", "tp"), "sp"),
        P(("fs", "tp"), "sp"),
    )
    out_specs = (P(("sp", "fs", "tp"), None), P(("fs", "tp"), "sp"))
    return jax.shard_map(
        per_device, mesh=mesh, in_specs=in_specs, out_specs=out_specs, check_vma=False
    )
```

profile of v0, /device:TPU:27, one launch (start us, length us, event | category | flops | bytes accessed | tf_op | source)
XLA Modules:
  0.0 261.1 jit_solution(7685932151415955385)
XLA Ops:
  7.3 1.1 fusion.33
  8.4 11.3 %psum.7 = f32[256]{0:T(256)S(1)} all-reduce(f32[256]{0:T(256)S(1)} %fusion.33), channel_id=1, replica_groups=mesh['sp'=4,'fs'=4,'tp'=2] {'fs','tp'}, use_global_device_ids=true, to_apply=%region_1.0 | all-reduce | flops 256 | bytes 2048 | tf_op jit(solution)/shard_map/psum | solution.py:219
  19.7 0.8 dynamic_slice.33
  20.4 1.7 fusion.35
  22.2 0.7 mul.191
  23.0 0.7 broadcast_in_dim.98
  23.7 0.8 copy.65
  24.5 11.9 %all_gather.35 = bf16[2048,64]{0,1:T(8,128)(2,1)} all-gather(bf16[512,64]{0,1:T(8,128)(2,1)} %param.25), channel_id=1, replica_groups=mesh['sp'=4,'fs'=4,'tp'=2] {'sp'}, dimensions={0}, use_global_device_ids=true | all-gather | bytes 327680 | tf_op jit(solution)/shard_map/all_gather | solution.py:245
  36.4 12.5 %all_gather.36 = bf16[2048,64]{0,1:T(8,128)(2,1)} all-gather(bf16[512,64]{0,1:T(8,128)(2,1)} %param.26), channel_id=1, replica_groups=mesh['sp'=4,'fs'=4,'tp'=2] {'sp'}, dimensions={0}, use_global_device_ids=true | all-gather | bytes 327680 | tf_op jit(solution)/shard_map/all_gather | solution.py:246
  48.9 13.4 %all_gather.34 = bf16[2048,128]{1,0:T(8,128)(2,1)S(1)} all-gather(bf16[512,128]{1,0:T(8,128)(2,1)S(1)} %copy-done.10), channel_id=1, replica_groups=mesh['sp'=4,'fs'=4,'tp'=2] {'sp'}, dimensions={0}, use_global_device_ids=true | all-gather | bytes 655360 | tf_op jit(solution)/shard_map/all_gather | solution.py:244
  62.3 13.0 %all_gather.38 = bf16[2048,128]{1,0:T(8,128)(2,1)S(1)} all-gather(bf16[512,128]{1,0:T(8,128)(2,1)S(1)} %copy-done.11), channel_id=1, replica_groups=mesh['sp'=4,'fs'=4,'tp'=2] {'sp'}, dimensions={0}, use_global_device_ids=true | all-gather | bytes 655360 | tf_op jit(solution)/shard_map/all_gather | solution.py:247
  75.3 13.5 %all_gather.39 = bf16[2048,128]{1,0:T(8,128)(2,1)S(1)} all-gather(bf16[512,128]{1,0:T(8,128)(2,1)S(1)} %copy-done.12), channel_id=1, replica_groups=mesh['sp'=4,'fs'=4,'tp'=2] {'sp'}, dimensions={0}, use_global_device_ids=true | all-gather | bytes 655360 | tf_op jit(solution)/shard_map/all_gather | solution.py:248
  88.8 13.2 %all_gather.40 = bf16[2048,128]{1,0:T(8,128)(2,1)S(1)} all-gather(bf16[512,128]{1,0:T(8,128)(2,1)S(1)} %copy-done.13), channel_id=1, replica_groups=mesh['sp'=4,'fs'=4,'tp'=2] {'sp'}, dimensions={0}, use_global_device_ids=true | all-gather | bytes 655360 | tf_op jit(solution)/shard_map/all_gather | solution.py:249
  102.0 14.1 %all_gather.37 = bf16[128,2048]{1,0:T(8,128)(2,1)} all-gather(bf16[128,512]{1,0:T(8,128)(2,1)S(1)} %copy-done.14), channel_id=1, replica_groups=mesh['sp'=4,'fs'=4,'tp'=2] {'sp'}, dimensions={1}, use_global_device_ids=true | all-gather | bytes 655360 | tf_op jit(solution)/shard_map/all_gather | solution.py:265
  116.1 12.9 %all_gather.43 = bf16[128,2048]{1,0:T(8,128)(2,1)} all-gather(bf16[128,512]{1,0:T(8,128)(2,1)S(1)} %copy-done.15), channel_id=1, replica_groups=mesh['sp'=4,'fs'=4,'tp'=2] {'sp'}, dimensions={1}, use_global_device_ids=true | all-gather | bytes 655360 | tf_op jit(solution)/shard_map/all_gather | solution.py:266
  129.1 0.8 broadcast_and_fusion
  129.9 1.8 convolution_convert_fusion.6
  131.7 1.7 convolution_convert_fusion.5
  133.4 0.4 convolution_convert_fusion.3
  134.0 0.4 convolution_convert_fusion.2
  134.4 0.4 convolution_convert_fusion.1
  134.8 0.4 convolution_convert_fusion
  135.7 1.4 fusion.29
  137.4 1.3 collective-permute-start
  139.6 35.9 %while.28 = (s32[]{:T(128)}, f32[2,128,64]{1,2,0:T(8,128)S(1)}, f32[8,2,32,128]{3,2,0,1:T(8,128)}, f32[8,2,32,64]{3,2,1,0:T(8,128)S(1)}, f32[8,2,32,64]{3,2,1,0:...) while((s32[]{:T(128)}, f32[2,128,64]{1,2,0:T(8,128)S(1)}, ...), condition=%wide.region_9.10_spmd.clone.clone, body=%wide.region_7.9_spmd.clone.clone.sunk | while | flops 50579456 | bytes 1623177 | solution.py:168
  143.1 0.3 fusion.229
  143.4 0.8 fusion.232
  147.5 0.3 fusion.229
  147.8 0.8 fusion.232
  152.0 0.3 fusion.229
  152.3 0.8 fusion.232
  156.5 0.3 fusion.229
  156.8 0.8 fusion.232
  161.0 0.3 fusion.229
  161.3 0.8 fusion.232
  165.5 0.3 fusion.229
  165.8 0.8 fusion.232
  169.9 0.3 fusion.229
  170.2 0.8 fusion.232
  174.4 0.3 fusion.229
  174.7 0.8 fusion.232
  175.5 10.7 %all-gather = bf16[8,128,64]{1,2,0:T(8,128)(2,1)S(1)} all-gather(bf16[2,128,64]{1,2,0:T(8,128)(2,1)S(1)} %convert_element_type.103), channel_id=2, replica_groups=mesh['sp'=4,'fs'=4,'tp'=2] {'sp'}, dimensions={0}, use_global_device_ids=true | all-gather | bytes 163840 | tf_op jit(solution)/shard_map/all_gather | solution.py:27
  186.3 1.2 while.27
  187.6 0.5 fusion.59
  190.3 0.5 fusion.44
  190.9 1.4 fusion.24
  192.3 0.7 fusion.55
  193.0 61.2 %reduce-scatter.2.cloned.1.call-done = bf16[32,2048]{1,0:T(8,128)(2,1)} async-done(((bf16[256,2048]{1,0:T(8,128)(2,1)}), bf16[32,2048]{1,0:T(8,128)(2,1)}) %reduce-scatter.2.cloned.1.call-update) | async-done | bytes 131088 | tf_op jit(solution)/shard_map/reduce_scatter | solution.py:268
  (310 shorter events, 31.4 us)
Async XLA Ops:
  7.2 128.5 %copy-start = (bf16[2048,64]{0,1:T(8,128)(2,1)S(1)}, bf16[2048,64]{0,1:T(8,128)(2,1)}, u32[]{:S(2)}) copy-start(bf16[2048,64]{0,1:T(8,128)(2,1)} %param.30) | copy-start | bytes 786436
  7.2 41.7 %copy-start.10 = (bf16[512,128]{1,0:T(8,128)(2,1)S(1)}, bf16[512,128]{1,0:T(8,128)(2,1)}, u32[]{:S(2)}) copy-start(bf16[512,128]{1,0:T(8,128)(2,1)} %param.24) | copy-start | bytes 393220
  7.2 55.1 %copy-start.11 = (bf16[512,128]{1,0:T(8,128)(2,1)S(1)}, bf16[512,128]{1,0:T(8,128)(2,1)}, u32[]{:S(2)}) copy-start(bf16[512,128]{1,0:T(8,128)(2,1)} %param.27) | copy-start | bytes 393220
  7.2 68.0 %copy-start.12 = (bf16[512,128]{1,0:T(8,128)(2,1)S(1)}, bf16[512,128]{1,0:T(8,128)(2,1)}, u32[]{:S(2)}) copy-start(bf16[512,128]{1,0:T(8,128)(2,1)} %param.28) | copy-start | bytes 393220
  7.2 81.6 %copy-start.13 = (bf16[512,128]{1,0:T(8,128)(2,1)S(1)}, bf16[512,128]{1,0:T(8,128)(2,1)}, u32[]{:S(2)}) copy-start(bf16[512,128]{1,0:T(8,128)(2,1)} %param.29) | copy-start | bytes 393220
  7.2 122.7 %all-gather.3.cloned.1.call-start = ((), (), s32[]{:S(2)}) async-start(), calls=%async_computation.1 | async-start | bytes 1179648 | tf_op jit(solution)/shard_map/all_gather | solution.py:225
  22.1 79.9 %copy-start.14 = (bf16[128,512]{1,0:T(8,128)(2,1)S(1)}, bf16[128,512]{1,0:T(8,128)(2,1)}, u32[]{:S(2)}) copy-start(bf16[128,512]{1,0:T(8,128)(2,1)} %param.38) | copy-start | bytes 393220
  22.1 232.1 %reduce-scatter.2.cloned.1.call-start = ((), (), s32[]{:S(2)}) async-start(), calls=%async_computation.2 | async-start | bytes 1179648 | tf_op jit(solution)/shard_map/reduce_scatter | solution.py:268
  23.0 93.1 %copy-start.2 = (f32[2,128,64]{1,2,0:T(8,128)}, f32[2,128,64]{1,2,0:T(8,128)S(1)}, u32[]{:S(2)}) copy-start(f32[2,128,64]{1,2,0:T(8,128)S(1)} %concatenate.37) | copy-start | bytes 196612
  23.7 92.4 %copy-start.15 = (bf16[128,512]{1,0:T(8,128)(2,1)S(1)}, bf16[128,512]{1,0:T(8,128)(2,1)}, u32[]{:S(2)}) copy-start(bf16[128,512]{1,0:T(8,128)(2,1)} %param.39) | copy-start | bytes 393220
  129.9 3.5 %copy-start.1 = (bf16[256,2048]{1,0:T(8,128)(2,1)S(1)}, bf16[256,2048]{1,0:T(8,128)(2,1)}, u32[]{:S(2)}) copy-start(bf16[256,2048]{1,0:T(8,128)(2,1)} %all-gather.3.cloned.1.call-done) | copy-start | bytes 3145732
  134.4 1.3 copy-start.7
  134.8 2.5 copy-start.17
  137.0 2.6 copy-start.4
  137.4 51.8 %collective-permute-start = (bf16[128,128]{0,1:T(8,128)(2,1)S(1)}, bf16[128,128]{0,1:T(8,128)(2,1)S(1)}, u32[]{:S(2)}, u32[]{:S(2)}) collective-permute-start(bf16[128,128]{0,1:T(8,128)(2,1)S(1)} %get-tuple-element.242), channel_id=1, source_target_pairs={{0,8},{8,16},{16,24},{1,9},{9,17},{17,25},{2,10},{10,18},{18,26},{... | collective-permute-start | bytes 98312 | tf_op jit(solution)/shard_map/ppermute | solution.py:22
  139.6 46.6 %copy-start.3 = (f32[2,128,64]{1,2,0:T(8,128)S(1)}, f32[2,128,64]{1,2,0:T(8,128)}, u32[]{:S(2)}) copy-start(f32[2,128,64]{1,2,0:T(8,128)} %copy-done.2) | copy-start | bytes 196612
  175.5 12.1 %copy-start.8 = (f32[8,2,32,128]{3,2,0,1:T(8,128)S(1)}, f32[8,2,32,128]{3,2,0,1:T(8,128)}, u32[]{:S(2)}) copy-start(f32[8,2,32,128]{3,2,0,1:T(8,128)} %get-tuple-element.157) | copy-start | bytes 786436
  175.5 13.1 %copy-start.18 = (f32[64]{0:T(128)S(1)}, f32[64]{0:T(128)}, u32[]{:S(2)}) copy-start(f32[64]{0:T(128)} %param.34) | copy-start | bytes 772
  187.5 1.8 copy-start.9
  187.5 2.1 copy-start.16
  189.2 1.0 copy-start.6
  189.8 1.1 copy-start.5
  189.8 1.1 copy-start.19
Sparse Core Ops, SparseCore 0:
  22.2 25.3 all-gather.2
  192.5 61.7 reduce-scatter.1
where the time goes:
time: 264 us; the launch traced here: 261 us
  blocking collectives  126 us (48%)
  waiting for transfers between devices  61.2 us (23%)
  matrix products  43.7 us (17%)
  between operations  14.6 us (6%)
  other arithmetic  6.77 us (3%)
  local copies, waits for them, and re-layouts  5.52 us (2%)
    reduce_scatter x1, waiting for transfers between devices, per_device(): lax.psum_scatter((jnp.dot(att_mix, att_full, preferred_element_type=jnp.f...  61.2 us
    all_gather x1, blocking collectives, per_device(): lax.all_gather(out_att_w, 'sp', axis=1, tiled=True)  14.1 us
    all_gather x1, blocking collectives, per_device(): lax.all_gather(rec_key_w, 'sp', axis=0, tiled=True)  13.5 us
    all_gather x1, blocking collectives, per_device(): lax.all_gather(query_w, 'sp', axis=0, tiled=True)  13.4 us
    all_gather x1, blocking collectives, per_device(): lax.all_gather(rec_value_w, 'sp', axis=0, tiled=True)  13.2 us
    all_gather x1, blocking collectives, per_device(): lax.all_gather(recept_w, 'sp', axis=0, tiled=True)  13 us
    all_gather x1, blocking collectives, per_device(): lax.all_gather(out_rec_w, 'sp', axis=1, tiled=True)  12.9 us
    all_gather x1, blocking collectives, per_device(): lax.all_gather(value_w, 'sp', axis=0, tiled=True)  12.5 us
  transfers between devices with their start and end apart: 3, of which 1 were waited for; matrix products, arithmetic and copies ran while one was open for 16% of the time, Pallas kernels for 0%

commit v1 on v0

--- a/solution.py
+++ b/solution.py
@@ -1,8 +1,11 @@
+import functools
 import math
 
 import jax
 import jax.numpy as jnp
 from jax import lax
+from jax.experimental import pallas as pl
+from jax.experimental.pallas import tpu as pltpu
 from jax.sharding import PartitionSpec as P
 
 HEAD = 64
@@ -277,7 +280,7 @@
     return (mixed_out, row_lse)
 
 
-def solution(mesh):
+def general(mesh):
     in_specs = (
         P("sp", ("fs", "tp")),
         P(),
@@ -302,3 +305,644 @@
     return jax.shard_map(
         per_device, mesh=mesh, in_specs=in_specs, out_specs=out_specs, check_vma=False
     )
+
+
+LANES = 128
+CHUNK = 64
+MESH = pl.DeviceIdType.MESH
+
+
+def dot(a, b):
+    return jnp.dot(a, b, preferred_element_type=jnp.float32)
+
+
+def dot_t(a, b, dims):
+    return lax.dot_general(a, b, (dims, ((), ())), preferred_element_type=jnp.float32)
+
+
+def halves(values):
+    high = values.astype(jnp.bfloat16)
+    return high, (values - high.astype(jnp.float32)).astype(jnp.bfloat16)
+
+
+def exact(a, b, dims=((1,), (0,))):
+    a_hi, a_lo = halves(a)
+    b_hi, b_lo = halves(b)
+    return dot_t(a_hi, b_hi, dims) + (dot_t(a_hi, b_lo, dims) + dot_t(a_lo, b_hi, dims))
+
+
+def layer_kernel(n_sp, n_fs, n_tp, *refs):
+    (tok, gain, recept_w, rec_key_w, rec_value_w, query_w, kv_w, out_att, out_rec) = refs[:9]
+    (down, up, base, rate, q_gain, k_gain, sink, g_gain, out, lse_out) = refs[9:19]
+    w_bufs = refs[19:26]
+    (tok_buf, hid, halo_out, halo_in, state_out, state_in, part, part_in) = refs[26:34]
+    (ward_out, ward_low, got, got_low) = refs[34:38]
+    (ring_send, ring_recv, chip_send, chip_recv, core_send, core_recv, ward_send, ward_recv,
+     one_send, one_recv, st_send, st_recv, red_send, red_recv) = refs[38:]
+    weights = (recept_w, rec_key_w, rec_value_w, query_w, kv_w, out_att, out_rec)
+    groups = n_fs * n_tp
+    place = lax.axis_index("sp")
+    own = lax.axis_index("fs") * n_tp + lax.axis_index("tp")
+    rows = tok.shape[0]
+
+    def peer(step):
+        other = lax.rem(own + step, groups)
+        return {"fs": lax.div(other, n_tp), "tp": lax.rem(other, n_tp)}
+
+    barrier = pltpu.get_barrier_semaphore()
+    for step in range(1, groups):
+        pl.semaphore_signal(barrier, inc=1, device_id=peer(step), device_id_type=MESH)
+    for step in range(1, n_sp):
+        pl.semaphore_signal(
+            barrier, inc=1, device_id={"sp": lax.rem(place + step, n_sp)}, device_id_type=MESH
+        )
+    pl.semaphore_wait(barrier, groups - 1 + n_sp - 1)
+
+    def hop(item, way, step):
+        sign = 1 if way == 0 else -1
+        src = weights[item] if step == 0 else w_bufs[item].at[lax.rem(place - sign * step + n_sp, n_sp)]
+        return pltpu.make_async_remote_copy(
+            src_ref=src,
+            dst_ref=w_bufs[item].at[lax.rem(place - sign * step + n_sp, n_sp)],
+            send_sem=ring_send.at[item, way, step],
+            recv_sem=ring_recv.at[item, way, step],
+            device_id={"sp": lax.rem(place + sign + n_sp, n_sp)},
+            device_id_type=MESH,
+        )
+
+    def inner(at):
+        return (at >= 1) & (at <= n_sp - 2)
+
+    inside = inner(place)
+    outside = ~inside
+    helps = inside & ((place == 1) | (place == n_sp - 2))
+    partner = jnp.where(
+        place == 0, 1, jnp.where(place == n_sp - 1, n_sp - 2, jnp.where(place == 1, 0, n_sp - 1))
+    )
+    inputs = 5
+
+    def sends(item, way, step):
+        if way == 0:
+            base_case, to = (place >= step) & (place + 1 < n_sp), place + 1
+        else:
+            base_case, to = (place + step < n_sp) & (place >= 1), place - 1
+        return base_case & inner(to) if item < inputs else base_case
+
+    def takes(item, way, step):
+        base_case = place >= step + 1 if way == 0 else place + step + 1 < n_sp
+        return base_case & inside if item < inputs else base_case
+
+    def start(items, step, to_inner):
+        for item in items:
+            for way in (0, 1):
+                to = inner(place + (1 if way == 0 else -1))
+
+                @pl.when(sends(item, way, step) & (to if to_inner else ~to))
+                def _():
+                    hop(item, way, step).start()
+
+    def sent(item, step):
+        for way in (0, 1):
+
+            @pl.when(sends(item, way, step))
+            def _():
+                hop(item, way, step).wait_send()
+
+    def relay(items, step, from_inner):
+        for item in items:
+            for way in (0, 1):
+                origin = inner(place - (1 if way == 0 else -1))
+                mine = inside & (origin if from_inner else ~origin)
+
+                @pl.when(takes(item, way, step) & mine)
+                def _():
+                    hop(item, way, step).wait_recv()
+
+                if step + 1 < n_sp - 1:
+
+                    @pl.when(sends(item, way, step + 1) & mine)
+                    def _():
+                        hop(item, way, step + 1).start()
+
+    rec_items, att_items, out_items = (0, 1, 2), (3, 4), (5, 6)
+
+    def ward_tok():
+        return pltpu.make_async_remote_copy(
+            src_ref=tok, dst_ref=tok_buf.at[1, own], send_sem=ward_send.at[0],
+            recv_sem=ward_recv.at[0], device_id={"sp": partner}, device_id_type=MESH,
+        )
+
+    fs_at, tp_at = lax.axis_index("fs"), lax.axis_index("tp")
+
+    def chip_copy(which, step):
+        return pltpu.make_async_remote_copy(
+            src_ref=tok if which == 0 else tok_buf.at[1, own], dst_ref=tok_buf.at[which, own],
+            send_sem=chip_send.at[which, step - 1], recv_sem=chip_recv.at[which, step - 1],
+            device_id={"fs": lax.rem(fs_at + step, n_fs)}, device_id_type=MESH,
+        )
+
+    def core_copy(which, step, turn):
+        slot = lax.rem(fs_at - step + n_fs, n_fs) * n_tp + tp_at
+        return pltpu.make_async_remote_copy(
+            src_ref=tok if which == 0 and step == 0 else tok_buf.at[which, slot],
+            dst_ref=tok_buf.at[which, slot],
+            send_sem=core_send.at[which, step, turn - 1], recv_sem=core_recv.at[which, step, turn - 1],
+            device_id={"tp": lax.rem(tp_at + turn, n_tp)}, device_id_type=MESH,
+        )
+
+    def to_chips(which):
+        for step in range(1, n_fs):
+            chip_copy(which, step).start()
+        for turn in range(1, n_tp):
+            core_copy(which, 0, turn).start()
+
+    def to_cores(which):
+        for step in range(1, n_fs):
+            chip_copy(which, step).wait_recv()
+            for turn in range(1, n_tp):
+                core_copy(which, step, turn).start()
+
+    def all_tokens(which):
+        for step in range(n_fs):
+            for turn in range(1, n_tp):
+                core_copy(which, step, turn).wait_recv()
+
+    width = tok.shape[1]
+
+    def input_norm(which):
+        squares = jnp.zeros((rows, 1), jnp.float32)
+        for group in range(groups):
+            values = tok_buf[which, group].astype(jnp.float32)
+            squares = squares + jnp.sum(values * values, axis=1, keepdims=True)
+        inv_rms = lax.rsqrt(squares / (width * groups) + NORM_EPS)
+        for group in range(groups):
+            cut = slice(group * width, (group + 1) * width)
+            hid[which, :, cut] = (
+                tok_buf[which, group].astype(jnp.float32) * inv_rms * gain[:, cut]
+            ).astype(jnp.bfloat16)
+
+    def project(which, item):
+        buf = w_bufs[item]
+        flat = buf[...].reshape(buf.shape[0] * buf.shape[1], buf.shape[2])
+        return dot(hid[which], flat).astype(jnp.bfloat16)
+
+    def low_rank(which):
+        return jnp.tanh(dot(hid[which], down[...])).astype(jnp.bfloat16)
+
+    def ward_copy(item):
+        source, target = (ward_low, got_low) if item == inputs else (ward_out.at[item], got.at[item])
+        return pltpu.make_async_remote_copy(
+            src_ref=source, dst_ref=target, send_sem=ward_send.at[1 + item],
+            recv_sem=ward_recv.at[1 + item], device_id={"sp": partner}, device_id_type=MESH,
+        )
+
+    @pl.when(outside)
+    def _():
+        ward_tok().start()
+
+    @pl.when(inside)
+    def _():
+        to_chips(0)
+
+    start(rec_items, 0, True)
+    start(out_items, 0, False)
+
+    @pl.when(outside)
+    def _():
+        start(att_items, 0, True)
+        start(out_items, 0, True)
+
+    tok_buf[0, own] = tok[...]
+    for item in range(len(weights)):
+        w_bufs[item][place] = weights[item][...]
+
+    @pl.when(place == 0)
+    def _():
+        halo_in[...] = jnp.zeros_like(halo_in)
+
+    @pl.when(helps)
+    def _():
+        ward_tok().wait_recv()
+        to_chips(1)
+
+    @pl.when(inside)
+    def _():
+        to_cores(0)
+
+    relay(rec_items[:2], 0, False)
+
+    @pl.when(inside)
+    def _():
+        all_tokens(0)
+        input_norm(0)
+
+    relay(rec_items[2:], 0, False)
+    relay(rec_items, 0, True)
+
+    @pl.when(inside)
+    def _():
+        start(att_items, 0, True)
+
+    @pl.when(helps)
+    def _():
+        to_cores(1)
+        all_tokens(1)
+        input_norm(1)
+
+    relay(att_items, 0, False)
+
+    @pl.when(inside)
+    def _():
+        start(out_items, 0, True)
+
+    for step in range(1, n_sp - 2):
+        relay(rec_items, step, True)
+
+    @pl.when(helps)
+    def _():
+        for item in rec_items:
+            ward_out[item] = project(1, item)
+        ward_low[...] = low_rank(1)
+
+    @pl.when(inside)
+    def _():
+        got_low[...] = low_rank(0)
+
+    @pl.when(helps)
+    def _():
+        for item in rec_items + (inputs,):
+            ward_copy(item).start()
+
+    @pl.when(inside)
+    def _():
+        for item in rec_items:
+            got[item] = project(0, item)
+
+    @pl.when(outside)
+    def _():
+        for item in rec_items + (inputs,):
+            ward_copy(item).wait_recv()
+
+    span = up.shape[1]
+    log_decay = -jnp.exp(dot(got_low[...], up[...]) + base[...])
+    reads = got[0].astype(jnp.float32)
+    keys = got[1].astype(jnp.float32)
+    vals = got[2].astype(jnp.float32)
+
+    chunks = rows // CHUNK
+    row_at = lax.broadcasted_iota(jnp.int32, (rows, rows), 0)
+    col_at = lax.broadcasted_iota(jnp.int32, (rows, rows), 1)
+    same = lax.div(row_at, CHUNK) == lax.div(col_at, CHUNK)
+    inclusive = same & (row_at >= col_at)
+    strict = same & (row_at > col_at)
+    ones = jnp.where(inclusive, 1.0, 0.0).astype(jnp.bfloat16)
+    ld_hi, ld_lo = halves(log_decay)
+    ld_rest = (log_decay - ld_hi.astype(jnp.float32) - ld_lo.astype(jnp.float32)).astype(jnp.bfloat16)
+    cum = dot(ones, ld_hi) + (dot(ones, ld_lo) + dot(ones, ld_rest))
+    cum_c = cum.reshape(chunks, CHUNK, span)
+    middle = cum_c[:, CHUNK // 2 - 1 : CHUNK // 2, :]
+    last = cum_c[:, CHUNK - 1 : CHUNK, :]
+    rel = (cum_c - middle).reshape(rows, span)
+    to_end = jnp.exp(last - cum_c).reshape(rows, span)
+    eye = jnp.where(
+        lax.broadcasted_iota(jnp.int32, (HEAD, HEAD), 0) == lax.broadcasted_iota(jnp.int32, (HEAD, HEAD), 1),
+        1.0, 0.0,
+    )
+    big_eye = jnp.where(row_at == col_at, 1.0, 0.0)
+    zeros = jnp.zeros((HEAD, HEAD), jnp.float32)
+    rec_heads = span // HEAD
+    from_start, own_part = [], []
+    for head in range(rec_heads):
+        at = slice(head * HEAD, (head + 1) * HEAD)
+        k, v, r = keys[:, at], vals[:, at], reads[:, at]
+        unit = k * lax.rsqrt(jnp.sum(k * k, axis=1, keepdims=True) + KEY_EPS)
+        write = unit * rate[:, at]
+        before = cum[:, at] - log_decay[:, at]
+        up_rel, down_rel = jnp.exp(rel[:, at]), jnp.exp(-rel[:, at])
+        left = jnp.concatenate([-unit * jnp.exp(rel[:, at] - log_decay[:, at]), r * up_rel], axis=0)
+        right = jnp.concatenate([write * down_rel, k * down_rel], axis=0)
+        table = exact(left, right, ((1,), (1,)))
+        m_ab = jnp.where(strict, table[:rows, :rows], 0.0)
+        m_ak = jnp.where(strict, table[:rows, rows:], 0.0)
+        m_rb = jnp.where(inclusive, table[rows:, :rows], 0.0)
+        m_rk = jnp.where(inclusive, table[rows:, rows:], 0.0)
+        inverse, power = big_eye + m_ab, m_ab
+        for _ in range(CHUNK.bit_length() - 2):
+            power = exact(power, power)
+            inverse = inverse + exact(inverse, power)
+        pu = exact(inverse, jnp.concatenate([-unit * jnp.exp(before), exact(m_ak, v)], axis=1))
+        mixed_pu = exact(m_rb, pu)
+        given = r * jnp.exp(cum[:, at]) + mixed_pu[:, :HEAD]
+        offset = mixed_pu[:, HEAD:] + exact(m_rk, v)
+        b_end, k_end = write * to_end[:, at], k * to_end[:, at]
+        pair = jnp.concatenate([eye, zeros], axis=1)
+        reach = []
+        for chunk in range(chunks):
+            cut = slice(chunk * CHUNK, (chunk + 1) * CHUNK)
+            reach.append(exact(given[cut], pair))
+            step_map = exact(b_end[cut], pu[cut], ((0,), (0,)))
+            turn = step_map[:, :HEAD] + eye * jnp.exp(last[chunk][:, at])
+            grown = step_map[:, HEAD:] + exact(k_end[cut], v[cut], ((0,), (0,)))
+            pair = exact(turn, pair) + jnp.concatenate([zeros, grown], axis=1)
+        reach = jnp.concatenate(reach, axis=0)
+        from_start.append(reach[:, :HEAD])
+        own_part.append(reach[:, HEAD:] + offset)
+        state_out[head] = pair.astype(jnp.bfloat16)
+        if head == 0:
+            relay(out_items, 0, False)
+
+    def state_copy(step):
+        return pltpu.make_async_remote_copy(
+            src_ref=state_out, dst_ref=state_in.at[place], send_sem=st_send.at[step - 1],
+            recv_sem=st_recv.at[step - 1], device_id={"sp": lax.rem(place + step, n_sp)},
+            device_id_type=MESH,
+        )
+
+    for step in range(n_sp - 2):
+        relay(att_items, step, True)
+    for step in range(1, n_sp):
+        @pl.when(place + step < n_sp)
+        def _():
+            state_copy(step).start()
+
+    @pl.when(helps)
+    def _():
+        for item in att_items:
+            ward_out[item] = project(1, item)
+
+    @pl.when(inside)
+    def _():
+        for item in att_items:
+            got[item] = project(0, item)
+
+    @pl.when(helps)
+    def _():
+        for item in att_items:
+            ward_copy(item).start()
+
+    relay(out_items, 0, True)
+
+    @pl.when(outside)
+    def _():
+        for item in att_items:
+            ward_copy(item).wait_recv()
+
+    q_all = got[3].astype(jnp.float32)
+    kv_all = got[4].astype(jnp.float32)
+    kv_heads = kv_all.shape[1] // (2 * HEAD)
+    q_heads = q_all.shape[1] // HEAD
+    share = q_heads // kv_heads
+
+    def normed(values, gain_ref):
+        mean_sq = jnp.mean(values * values, axis=1, keepdims=True)
+        return (values * lax.rsqrt(mean_sq + NORM_EPS) * gain_ref[...]).astype(jnp.bfloat16)
+
+    key_n = [normed(kv_all[:, h * HEAD : (h + 1) * HEAD], k_gain) for h in range(kv_heads)]
+    value_n = [
+        kv_all[:, (kv_heads + h) * HEAD : (kv_heads + h + 1) * HEAD].astype(jnp.bfloat16)
+        for h in range(kv_heads)
+    ]
+    halo_out[...] = jnp.concatenate([x[rows - WINDOW :] for x in key_n + value_n], axis=1)
+    query_n = [normed(q_all[:, h * HEAD : (h + 1) * HEAD], q_gain) for h in range(q_heads)]
+
+    def halo_copy():
+        return pltpu.make_async_remote_copy(
+            src_ref=halo_out, dst_ref=halo_in, send_sem=one_send.at[0], recv_sem=one_recv.at[0],
+            device_id={"sp": lax.rem(place + 1, n_sp)}, device_id_type=MESH,
+        )
+
+    @pl.when(place + 1 < n_sp)
+    def _():
+        halo_copy().start()
+
+    blocks = rows // WINDOW
+    lag = (
+        lax.broadcasted_iota(jnp.int32, (WINDOW, 2 * WINDOW), 0)
+        + WINDOW
+        - lax.broadcasted_iota(jnp.int32, (WINDOW, 2 * WINDOW), 1)
+    )
+    key_col = lax.broadcasted_iota(jnp.int32, (WINDOW, 2 * WINDOW), 1)
+    mixes = [[None] * q_heads for _ in range(blocks)]
+
+    def attend_block(block, band_keys, band_values):
+        allowed = (lag >= 0) & (lag < WINDOW)
+        if block == 0:
+            allowed = allowed & (key_col + (place * blocks - 1) * WINDOW >= 0)
+        cut = slice(block * WINDOW, (block + 1) * WINDOW)
+        for h in range(q_heads):
+            top_sink = sink[0, h]
+            scores = dot_t(query_n[h][cut], band_keys[h // share], ((1,), (1,))) * (1.0 / math.sqrt(HEAD))
+            masked = jnp.where(allowed, scores, -jnp.inf)
+            top = jnp.maximum(jnp.max(masked, axis=1, keepdims=True), top_sink)
+            weight = jnp.where(allowed, jnp.exp(masked - top), 0.0)
+            total = jnp.sum(weight, axis=1, keepdims=True) + jnp.exp(top_sink - top)
+            spread = jnp.broadcast_to(top + jnp.log(total), (WINDOW, LANES)).T
+            lse_out[h : h + 1, cut] = spread[0:1]
+            probs = (weight / total).astype(jnp.bfloat16)
+            mixes[block][h] = dot(probs, band_values[h // share]).astype(jnp.bfloat16)
+
+    for block in range(1, blocks):
+        band = slice((block - 1) * WINDOW, (block + 1) * WINDOW)
+        attend_block(block, [x[band] for x in key_n], [x[band] for x in value_n])
+
+    @pl.when(place >= 1)
+    def _():
+        halo_copy().wait_recv()
+
+    halo = halo_in[...]
+    before_k = [halo[:, h * HEAD : (h + 1) * HEAD] for h in range(kv_heads)]
+    before_v = [halo[:, (kv_heads + h) * HEAD : (kv_heads + h + 1) * HEAD] for h in range(kv_heads)]
+    attend_block(
+        0,
+        [jnp.concatenate([b, x[:WINDOW]], axis=0) for b, x in zip(before_k, key_n)],
+        [jnp.concatenate([b, x[:WINDOW]], axis=0) for b, x in zip(before_v, value_n)],
+    )
+    att_mix = jnp.concatenate([jnp.concatenate(line, axis=1) for line in mixes], axis=0)
+    for step in range(1, n_sp - 2):
+        relay(out_items, step, True)
+
+    @pl.when(outside)
+    def _():
+        for item in out_items:
+            for step in range(n_sp - 1):
+                for way in (0, 1):
+
+                    @pl.when(takes(item, way, step))
+                    def _():
+                        hop(item, way, step).wait_recv()
+
+    for step in range(1, n_sp):
+        @pl.when(place >= step)
+        def _():
+            state_copy(step).wait_recv()
+    rec_parts = []
+    for head in range(rec_heads):
+        state = zeros
+        for k in range(n_sp - 1):
+            pair = state_in[k, head].astype(jnp.float32)
+            moved = exact(pair[:, :HEAD], state) + pair[:, HEAD:]
+            state = jnp.where(place > k, moved, state)
+        result = own_part[head] + exact(from_start[head], state)
+        mean_val = jnp.mean(result, axis=1, keepdims=True)
+        centered = result - mean_val
+        variance = jnp.mean(centered * centered, axis=1, keepdims=True)
+        at = slice(head * HEAD, (head + 1) * HEAD)
+        rec_parts.append((centered * lax.rsqrt(variance + GROUP_EPS) * g_gain[:, at]).astype(jnp.bfloat16))
+    rec_mix = jnp.concatenate(rec_parts, axis=1)
+
+    cols = out_att.shape[1]
+    few = rows // groups
+    for k in range(n_sp):
+        block = (dot(att_mix, w_bufs[5][k]) + dot(rec_mix, w_bufs[6][k])).astype(jnp.bfloat16)
+        part[:, :, k * cols : (k + 1) * cols] = block.reshape(groups, few, cols)
+
+    def red_copy(step):
+        return pltpu.make_async_remote_copy(
+            src_ref=part.at[lax.rem(own + step, groups)], dst_ref=part_in.at[step - 1],
+            send_sem=red_send.at[step - 1], recv_sem=red_recv.at[step - 1],
+            device_id=peer(step), device_id_type=MESH,
+        )
+
+    for step in range(1, groups):
+        red_copy(step).start()
+    @pl.when(outside)
+    def _():
+        ward_tok().wait_send()
+
+    def tokens_sent(which):
+        for step in range(1, n_fs):
+            chip_copy(which, step).wait_send()
+        for step in range(n_fs):
+            for turn in range(1, n_tp):
+                core_copy(which, step, turn).wait_send()
+
+    @pl.when(inside)
+    def _():
+        tokens_sent(0)
+
+    @pl.when(helps)
+    def _():
+        tokens_sent(1)
+        for item in range(inputs + 1):
+            ward_copy(item).wait_send()
+
+    for item in range(len(weights)):
+        for step in range(n_sp - 1):
+            sent(item, step)
+    for step in range(1, n_sp):
+        @pl.when(place + step < n_sp)
+        def _():
+            state_copy(step).wait_send()
+
+    @pl.when(place + 1 < n_sp)
+    def _():
+        halo_copy().wait_send()
+
+    total = part[own].astype(jnp.float32)
+    for step in range(1, groups):
+        red_copy(step).wait_recv()
+        total = total + part_in[step - 1].astype(jnp.float32)
+    out[...] = total.astype(jnp.bfloat16)
+    for step in range(1, groups):
+        red_copy(step).wait_send()
+
+
+def in_kernel(
+    n_sp, n_fs, n_tp,
+    tokens, norm_gain, query_w, key_w, value_w, recept_w, rec_key_w, rec_value_w,
+    decay_down, decay_up, decay_base, learn_rate, query_gain, key_gain, sink_logit,
+    group_gain, out_att_w, out_rec_w,
+):
+    groups = n_fs * n_tp
+    rows, width = tokens.shape
+    rec_span = recept_w.shape[1]
+    model = width * groups
+    up = lax.dynamic_slice_in_dim(decay_up, lax.axis_index(("fs", "tp")) * rec_span, rec_span, 1)
+    base = jnp.repeat(decay_base.T, HEAD, axis=1)
+    kv_w = jnp.concatenate([key_w, value_w], axis=1)
+    weights = (recept_w, rec_key_w, rec_value_w, query_w, kv_w, out_att_w, out_rec_w)
+    vmem = pl.BlockSpec(memory_space=pltpu.VMEM)
+    smem = pl.BlockSpec(memory_space=pltpu.SMEM)
+    bf16 = jnp.bfloat16
+    heads = rec_span // HEAD
+    dma = pltpu.SemaphoreType.DMA
+    scratch = [pltpu.VMEM((n_sp, *w.shape), bf16) for w in weights] + [
+        pltpu.VMEM((2, groups, rows, width), bf16),
+        pltpu.VMEM((2, rows, model), bf16),
+        pltpu.VMEM((WINDOW, kv_w.shape[1]), bf16),
+        pltpu.VMEM((WINDOW, kv_w.shape[1]), bf16),
+        pltpu.VMEM((heads, HEAD, 2 * HEAD), bf16),
+        pltpu.VMEM((n_sp, heads, HEAD, 2 * HEAD), bf16),
+        pltpu.VMEM((groups, rows // groups, model), bf16),
+        pltpu.VMEM((groups - 1, rows // groups, model), bf16),
+        pltpu.VMEM((5, rows, rec_span), bf16),
+        pltpu.VMEM((rows, decay_down.shape[1]), bf16),
+        pltpu.VMEM((5, rows, rec_span), bf16),
+        pltpu.VMEM((rows, decay_down.shape[1]), bf16),
+        dma((len(weights), 2, n_sp - 1)),
+        dma((len(weights), 2, n_sp - 1)),
+        dma((2, n_fs - 1)),
+        dma((2, n_fs - 1)),
+        dma((2, n_fs, n_tp - 1)),
+        dma((2, n_fs, n_tp - 1)),
+        dma((7,)),
+        dma((7,)),
+        dma((1,)),
+        dma((1,)),
+        dma((n_sp - 1,)),
+        dma((n_sp - 1,)),
+        dma((groups - 1,)),
+        dma((groups - 1,)),
+    ]
+    return pl.pallas_call(
+        functools.partial(layer_kernel, n_sp, n_fs, n_tp),
+        out_shape=(
+            jax.ShapeDtypeStruct((rows // groups, model), bf16),
+            jax.ShapeDtypeStruct((sink_logit.shape[0], rows), jnp.float32),
+        ),
+        in_specs=[vmem] * 15 + [smem] + [vmem],
+        out_specs=(vmem, vmem),
+        scratch_shapes=scratch,
+        compiler_params=pltpu.CompilerParams(
+            collective_id=0, has_side_effects=True, vmem_limit_bytes=60 * 1024 * 1024
+        ),
+    )(
+        tokens, norm_gain[None], *weights, decay_down, up, base, learn_rate[None],
+        query_gain[None], key_gain[None], sink_logit[None], group_gain[None],
+    )
+
+
+def solution(mesh):
+    n_sp, n_fs, n_tp = (mesh.shape[name] for name in ("sp", "fs", "tp"))
+    plain = general(mesh)
+
+    def layer(*arrays):
+        if (arrays[-1].shape[1] // n_sp) % LANES or n_sp > LANES // 8 or n_sp < 4:
+            return plain(*arrays)
+        in_specs = (
+            P("sp", ("fs", "tp")),
+            P(),
+            P("sp", ("fs", "tp")),
+            P("sp", ("fs", "tp")),
+            P("sp", ("fs", "tp")),
+            P("sp", ("fs", "tp")),
+            P("sp", ("fs", "tp")),
+            P("sp", ("fs", "tp")),
+            P(),
+            P(),
+            P(("fs", "tp"), "sp"),
+            P(("fs", "tp")),
+            P(),
+            P(),
+            P(("fs", "tp")),
+            P(("fs", "tp")),
+            P(("fs", "tp"), "sp"),
+            P(("fs", "tp"), "sp"),
+        )
+        out_specs = (P(("sp", "fs", "tp"), None), P(("fs", "tp"), "sp"))
+        return jax.shard_map(
+            functools.partial(in_kernel, n_sp, n_fs, n_tp),
+            mesh=mesh, in_specs=in_specs, out_specs=out_specs, check_vma=False,
+        )(*arrays)
+
+    return layer

time: 264 us -> 78.5 us (0.30); the launches traced: 261 us -> 78.3 us
  blocking collectives: 126 us -> 0 us
  Pallas kernels: 0 us -> 70.3 us
  waiting for transfers between devices: 61.2 us -> 0 us
  matrix products: 43.7 us -> 0 us
  between operations: 14.6 us -> 0.7 us
  other arithmetic: 6.77 us -> 0.77 us
    all_gather x9 -> x0, blocking collectives: 115 us -> none  [the longest x1 14.1 us: per_device(): lax.all_gather(out_att_w, 'sp', axis=1, tiled=True)]
    pallas_call x0 -> x1, Pallas kernels: none -> 70.3 us  [in_kernel(): pl.pallas_call(functools.partial(layer_kernel, n_sp, n_fs, n_tp), out_sha...]
    reduce_scatter x1 -> x0, waiting for transfers between devices: 61.2 us -> none  [per_device(): lax.psum_scatter((jnp.dot(att_mix, att_full, preferred_element_type=jnp.f...]
    dot_general x176 -> x0, matrix products: 43.7 us -> none  [the longest x8 6.26 us: block_step(): jnp.einsum('hij,hjm->him', m_rk, current_value, precision=EXACT_PRECISION)]
    psum x1 -> x0, blocking collectives: 11.3 us -> none  [per_device(): squares = lax.psum(jnp.sum(own_values * own_values, axis=1), ('fs', 'tp'))]
    unnamed x40 -> x17, local copies, waits for them, and re-layouts: 0.38 us -> 5.19 us
  transfers between devices with their start and end apart: 3 -> 0, of which waited for: 1 -> 0; matrix products, arithmetic and copies ran while one was open for 16% -> 0% of each run, Pallas kernels for 0% -> 0%
where the time goes in v1:
time: 78.5 us; the launch traced here: 78.3 us
  Pallas kernels  70.3 us (90%)
  local copies, waits for them, and re-layouts  6.55 us (8%)
    pallas_call x1, Pallas kernels, in_kernel(): pl.pallas_call(functools.partial(layer_kernel, n_sp, n_fs, n_tp), out_sha...  70.3 us
    unnamed x17, local copies, waits for them, and re-layouts  5.19 us

profile of v1, /device:TPU:27, one launch (start us, length us, event | category | flops | bytes accessed | tf_op | source)
XLA Modules:
  0.0 78.3 jit_solution(2754217363405319191)
XLA Ops:
  0.6 0.0 copy-start
  0.6 0.0 copy-start.2
  0.7 0.9 %copy-done = bf16[64,1024]{1,0:T(8,128)(2,1)S(1)} copy-done((bf16[64,1024]{1,0:T(8,128)(2,1)S(1)}, bf16[64,1024]{1,0:T(8,128)(2,1)}, u32[]{:S(2)}) %copy-start) | copy-done | bytes 131096
  1.5 0.6 constant_dynamic-slice_fusion.refs_10_
  2.1 0.0 copy-done.2
  2.2 0.0 copy-start.3
  2.2 0.1 copy.24
  2.3 0.7 copy-done.3
  3.0 0.1 copy.25
  3.1 0.0 copy-start.4
  3.1 0.8 pad_maximum_fusion.refs_6_
  3.9 0.0 copy-done.4
  3.9 0.0 copy-start.1
  3.9 0.7 copy.27.refs_11_
  4.7 0.2 copy-done.1
  4.8 1.0 %copy.26.refs_9_ = bf16[2048,64]{1,0:T(8,128)(2,1)} copy(bf16[2048,64]{0,1:T(8,128)(2,1)S(1)} %copy-done.1) | data formatting | bytes 524288 | tf_op args[8]
  5.8 70.3 %shard_map.185 = (bf16[32,2048]{1,0:T(8,128)(2,1)}, f32[2,256]{1,0:T(2,128)}) custom-call(bf16[256,256]{1,0:T(8,128)(2,1)} %refs_0_.1, f32[1,2048]{1,0:T(1,128)} %bitcast.9, bf16[512,128]{1,0:T(8,128)(2,1)} %refs_2_.1, bf16[512,128]{1,0:T(8,128)(2,1)} %refs_3_.1, bf16[512,128]{1,0:T(8,128)(2,1)} %refs_4_.1, bf16[512,128]{1,0:T(8,128)(2,1)} %refs_5_.1, ...), custom_call_target="tpu_custom_call" | custom-call | tf_op jit(solution)/shard_map/pallas_call | solution.py:897
  76.1 0.0 copy-start.5
  76.1 1.6 %copy.30 = bf16[32,2048]{1,0:T(8,128)(2,1)} copy(bf16[32,2048]{1,0:T(8,128)(2,1)} %get-tuple-element.4) | data formatting | bytes 262144
  77.7 0.0 copy-done.5
  77.7 0.6 copy.31
  (1 shorter events, 0.0 us)
Async XLA Ops:
  0.6 0.9 %copy-start = (bf16[64,1024]{1,0:T(8,128)(2,1)S(1)}, bf16[64,1024]{1,0:T(8,128)(2,1)}, u32[]{:S(2)}) copy-start(bf16[64,1024]{1,0:T(8,128)(2,1)} %param.27) | copy-start | bytes 393220
  0.6 1.5 %copy-start.2 = (bf16[512,64]{0,1:T(8,128)(2,1)S(1)}, bf16[512,64]{0,1:T(8,128)(2,1)}, u32[]{:S(2)}) copy-start(bf16[512,64]{0,1:T(8,128)(2,1)} %param.21) | copy-start | bytes 196612
  2.2 0.8 %copy-start.3 = (bf16[512,64]{0,1:T(8,128)(2,1)S(1)}, bf16[512,64]{0,1:T(8,128)(2,1)}, u32[]{:S(2)}) copy-start(bf16[512,64]{0,1:T(8,128)(2,1)} %param.22) | copy-start | bytes 196612
  3.1 0.8 copy-start.4
  3.9 1.0 %copy-start.1 = (bf16[2048,64]{0,1:T(8,128)(2,1)S(1)}, bf16[2048,64]{0,1:T(8,128)(2,1)}, u32[]{:S(2)}) copy-start(bf16[2048,64]{0,1:T(8,128)(2,1)} %param.26) | copy-start | bytes 786436
  76.1 1.6 %copy-start.5 = (f32[2,256]{1,0:T(2,128)S(1)}, f32[2,256]{1,0:T(2,128)}, u32[]{:S(2)}) copy-start(f32[2,256]{1,0:T(2,128)} %get-tuple-element.5) | copy-start | bytes 6148

commit v2 on v1

--- a/solution.py
+++ b/solution.py
@@ -336,9 +336,9 @@
     (down, up, base, rate, q_gain, k_gain, sink, g_gain, out, lse_out) = refs[9:19]
     w_bufs = refs[19:26]
     (tok_buf, hid, halo_out, halo_in, state_out, state_in, part, part_in) = refs[26:34]
-    (ward_out, ward_low, got, got_low) = refs[34:38]
+    (ward_out, ward_low, got, got_low, pair_in, pair_sum) = refs[34:40]
     (ring_send, ring_recv, chip_send, chip_recv, core_send, core_recv, ward_send, ward_recv,
-     one_send, one_recv, st_send, st_recv, red_send, red_recv) = refs[38:]
+     one_send, one_recv, st_send, st_recv, red_send, red_recv, pair_send, pair_recv) = refs[40:]
     weights = (recept_w, rec_key_w, rec_value_w, query_w, kv_w, out_att, out_rec)
     groups = n_fs * n_tp
     place = lax.axis_index("sp")
@@ -583,8 +583,9 @@
         for item in rec_items + (inputs,):
             ward_copy(item).wait_recv()
 
-    span = up.shape[1]
-    log_decay = -jnp.exp(dot(got_low[...], up[...]) + base[...])
+    span = recept_w.shape[1]
+    up_cols = up[:, pl.ds(pl.multiple_of(own * span, LANES), span)]
+    log_decay = -jnp.exp(dot(got_low[...], up_cols) + base[...])
     reads = got[0].astype(jnp.float32)
     keys = got[1].astype(jnp.float32)
     vals = got[2].astype(jnp.float32)
@@ -794,16 +795,40 @@
     few = rows // groups
     for k in range(n_sp):
         block = (dot(att_mix, w_bufs[5][k]) + dot(rec_mix, w_bufs[6][k])).astype(jnp.bfloat16)
-        part[:, :, k * cols : (k + 1) * cols] = block.reshape(groups, few, cols)
+        for group in range(groups):
+            part[group % n_tp, group // n_tp, :, k * cols : (k + 1) * cols] = block[
+                group * few : (group + 1) * few
+            ]
+
+    def pair_copy(step, turn):
+        to = lax.rem(tp_at + turn, n_tp)
+        chip = lax.rem(fs_at + step, n_fs)
+        return pltpu.make_async_remote_copy(
+            src_ref=part.at[to, chip], dst_ref=pair_in.at[turn - 1, step],
+            send_sem=pair_send.at[step, turn - 1], recv_sem=pair_recv.at[step, turn - 1],
+            device_id={"tp": to}, device_id_type=MESH,
+        )
 
     def red_copy(step):
         return pltpu.make_async_remote_copy(
-            src_ref=part.at[lax.rem(own + step, groups)], dst_ref=part_in.at[step - 1],
+            src_ref=pair_sum.at[step - 1], dst_ref=part_in.at[step - 1],
             send_sem=red_send.at[step - 1], recv_sem=red_recv.at[step - 1],
-            device_id=peer(step), device_id_type=MESH,
-        )
-
-    for step in range(1, groups):
+            device_id={"fs": lax.rem(fs_at + step, n_fs)}, device_id_type=MESH,
+        )
+
+    def chip_total(step):
+        value = part[tp_at, lax.rem(fs_at + step, n_fs)].astype(jnp.float32)
+        for turn in range(1, n_tp):
+            pair_copy(step, turn).wait_recv()
+            value = value + pair_in[turn - 1, step].astype(jnp.float32)
+        return value
+
+    order = [*range(n_fs - 1, 0, -1), 0]
+    for step in order:
+        for turn in range(1, n_tp):
+            pair_copy(step, turn).start()
+    for step in order[:-1]:
+        pair_sum[step - 1] = chip_total(step).astype(jnp.bfloat16)
         red_copy(step).start()
     @pl.when(outside)
     def _():
@@ -838,13 +863,16 @@
     def _():
         halo_copy().wait_send()
 
-    total = part[own].astype(jnp.float32)
-    for step in range(1, groups):
+    total = chip_total(0)
+    for step in order[:-1]:
         red_copy(step).wait_recv()
         total = total + part_in[step - 1].astype(jnp.float32)
     out[...] = total.astype(jnp.bfloat16)
-    for step in range(1, groups):
-        red_copy(step).wait_send()
+    for step in range(n_fs):
+        for turn in range(1, n_tp):
+            pair_copy(step, turn).wait_send()
+        if step:
+            red_copy(step).wait_send()
 
 
 def in_kernel(
@@ -857,7 +885,6 @@
     rows, width = tokens.shape
     rec_span = recept_w.shape[1]
     model = width * groups
-    up = lax.dynamic_slice_in_dim(decay_up, lax.axis_index(("fs", "tp")) * rec_span, rec_span, 1)
     base = jnp.repeat(decay_base.T, HEAD, axis=1)
     kv_w = jnp.concatenate([key_w, value_w], axis=1)
     weights = (recept_w, rec_key_w, rec_value_w, query_w, kv_w, out_att_w, out_rec_w)
@@ -873,12 +900,14 @@
         pltpu.VMEM((WINDOW, kv_w.shape[1]), bf16),
         pltpu.VMEM((heads, HEAD, 2 * HEAD), bf16),
         pltpu.VMEM((n_sp, heads, HEAD, 2 * HEAD), bf16),
-        pltpu.VMEM((groups, rows // groups, model), bf16),
-        pltpu.VMEM((groups - 1, rows // groups, model), bf16),
+        pltpu.VMEM((n_tp, n_fs, rows // groups, model), bf16),
+        pltpu.VMEM((n_fs - 1, rows // groups, model), bf16),
         pltpu.VMEM((5, rows, rec_span), bf16),
         pltpu.VMEM((rows, decay_down.shape[1]), bf16),
         pltpu.VMEM((5, rows, rec_span), bf16),
         pltpu.VMEM((rows, decay_down.shape[1]), bf16),
+        pltpu.VMEM((n_tp - 1, n_fs, rows // groups, model), bf16),
+        pltpu.VMEM((n_fs - 1, rows // groups, model), bf16),
         dma((len(weights), 2, n_sp - 1)),
         dma((len(weights), 2, n_sp - 1)),
         dma((2, n_fs - 1)),
@@ -891,8 +920,10 @@
         dma((1,)),
         dma((n_sp - 1,)),
         dma((n_sp - 1,)),
-        dma((groups - 1,)),
-        dma((groups - 1,)),
+        dma((n_fs - 1,)),
+        dma((n_fs - 1,)),
+        dma((n_fs, n_tp - 1)),
+        dma((n_fs, n_tp - 1)),
     ]
     return pl.pallas_call(
         functools.partial(layer_kernel, n_sp, n_fs, n_tp),
@@ -907,7 +938,7 @@
             collective_id=0, has_side_effects=True, vmem_limit_bytes=60 * 1024 * 1024
         ),
     )(
-        tokens, norm_gain[None], *weights, decay_down, up, base, learn_rate[None],
+        tokens, norm_gain[None], *weights, decay_down, decay_up, base, learn_rate[None],
         query_gain[None], key_gain[None], sink_logit[None], group_gain[None],
     )
 

time: 78.5 us -> 75 us (0.955); the launches traced: 78.3 us -> 74 us
  Pallas kernels: 70.3 us -> 67.3 us
  local copies, waits for them, and re-layouts: 6.55 us -> 5.22 us
    pallas_call x1, Pallas kernels: 70.3 us -> 67.3 us  [in_kernel(): pl.pallas_call(functools.partial(layer_kernel, n_sp, n_fs, n_tp), out_sha...]
    unnamed x17 -> x13, local copies, waits for them, and re-layouts: 5.19 us -> 4.46 us
where the time goes in v2:
time: 75 us; the launch traced here: 74 us
  Pallas kernels  67.3 us (90%)
  local copies, waits for them, and re-layouts  5.22 us (7%)
  other arithmetic  0.77 us (1%)
    pallas_call x1, Pallas kernels, in_kernel(): pl.pallas_call(functools.partial(layer_kernel, n_sp, n_fs, n_tp), out_sha...  67.3 us
    unnamed x13, local copies, waits for them, and re-layouts  4.46 us

profile of v2, /device:TPU:27, one launch (start us, length us, event | category | flops | bytes accessed | tf_op | source)
XLA Modules:
  0.0 74.0 jit_solution(11024257864602460318)
XLA Ops:
  0.6 0.0 copy-start.1
  0.6 1.0 %copy.24 = bf16[512,64]{1,0:T(8,128)(2,1)S(1)} copy(bf16[512,64]{0,1:T(8,128)(2,1)} %param.21) | data formatting | bytes 131072 | tf_op args[3]
  1.6 0.0 copy-done.1
  1.6 0.1 copy.25
  1.8 0.0 copy-start.2
  1.8 0.8 %pad_maximum_fusion.refs_6_ = bf16[512,128]{1,0:T(8,128)(2,1)} fusion(bf16[512,64]{1,0:T(8,128)(2,1)S(1)} %copy.25, bf16[512,64]{1,0:T(8,128)(2,1)S(1)} %copy.24), kind=kLoop, calls=%fused_computation | loop fusion | flops 262144 | bytes 262144 | tf_op jit(solution)/shard_map/concatenate | solution.py:889
  2.5 0.0 copy-done.2
  2.5 0.0 copy-start
  2.6 0.7 %copy.27.refs_11_ = f32[256,128]{1,0:T(8,128)} copy(f32[256,128]{0,1:T(8,128)S(1)} %bitcast.8) | data formatting | bytes 262144 | tf_op jit(solution)/shard_map/reshape | solution.py:888
  3.3 0.2 copy-done
  3.5 1.0 %copy.26.refs_9_ = bf16[2048,64]{1,0:T(8,128)(2,1)} copy(bf16[2048,64]{0,1:T(8,128)(2,1)S(1)} %copy-done) | data formatting | bytes 524288 | tf_op args[8]
  4.5 67.3 %shard_map.185 = (bf16[32,2048]{1,0:T(8,128)(2,1)}, f32[2,256]{1,0:T(2,128)}) custom-call(bf16[256,256]{1,0:T(8,128)(2,1)} %refs_0_.1, f32[1,2048]{1,0:T(1,128)} %bitcast.9, bf16[512,128]{1,0:T(8,128)(2,1)} %refs_2_.1, bf16[512,128]{1,0:T(8,128)(2,1)} %refs_3_.1, bf16[512,128]{1,0:T(8,128)(2,1)} %refs_4_.1, bf16[512,128]{1,0:T(8,128)(2,1)} %refs_5_.1, ...), custom_call_target="tpu_custom_call" | custom-call | tf_op jit(solution)/shard_map/pallas_call | solution.py:928
  71.8 0.0 copy-start.3
  71.8 1.6 %copy.30 = bf16[32,2048]{1,0:T(8,128)(2,1)} copy(bf16[32,2048]{1,0:T(8,128)(2,1)} %get-tuple-element.4) | data formatting | bytes 262144
  73.4 0.0 copy-done.3
  73.4 0.6 copy.31
  (1 shorter events, 0.0 us)
Async XLA Ops:
  0.6 1.0 %copy-start.1 = (bf16[512,64]{0,1:T(8,128)(2,1)S(1)}, bf16[512,64]{0,1:T(8,128)(2,1)}, u32[]{:S(2)}) copy-start(bf16[512,64]{0,1:T(8,128)(2,1)} %param.22) | copy-start | bytes 196612
  1.8 0.8 %copy-start.2 = (f32[2,256]{1,0:T(2,128)S(1)}, f32[2,256]{1,0:T(2,128)}, u32[]{:S(2)}) copy-start(f32[2,256]{1,0:T(2,128)} %param.28) | copy-start | bytes 6148
  2.5 1.0 %copy-start = (bf16[2048,64]{0,1:T(8,128)(2,1)S(1)}, bf16[2048,64]{0,1:T(8,128)(2,1)}, u32[]{:S(2)}) copy-start(bf16[2048,64]{0,1:T(8,128)(2,1)} %param.26) | copy-start | bytes 786436
  71.8 1.6 %copy-start.3 = (f32[2,256]{1,0:T(2,128)S(1)}, f32[2,256]{1,0:T(2,128)}, u32[]{:S(2)}) copy-start(f32[2,256]{1,0:T(2,128)} %get-tuple-element.5) | copy-start | bytes 6148
